TPU v7x, 32 devices: a whole 2x2x4 slice. The times are simulated.
32 devices in a mesh: sp: 16 (over z, y, x), tp: 2 (over core).
Axes of the slice: x: 2, y: 2, z: 4, core: 2. Of those that a mesh axis runs over, the one named last changes fastest.
Arguments:
- tokens: bfloat16 [8192, 2048], P('sp', 'tp'), may hold values from -6 to 6
- norm_gain: float32 [2048], replicated, may hold values from 0.1 to 1.9
- outer_gate: bfloat16 [2048, 1024], P('sp', 'tp'), may hold values from -0.125 to 0.125
- inner_gate: bfloat16 [2048, 1024], P('sp', 'tp'), may hold values from -0.125 to 0.125
- conv_input: bfloat16 [2048, 1024], P('sp', 'tp'), may hold values from -0.125 to 0.125
- query_proj: bfloat16 [2048, 1024], P('sp', 'tp'), may hold values from -0.125 to 0.125
- key_proj: bfloat16 [2048, 1024], P('sp', 'tp'), may hold values from -0.125 to 0.125
- value_proj: bfloat16 [2048, 1024], P('sp', 'tp'), may hold values from -0.125 to 0.125
- out_gate: bfloat16 [2048, 1024], P('sp', 'tp'), may hold values from -0.125 to 0.125
- conv_taps: float32 [3, 1024], P(None, 'tp'), may hold values from -3.5 to 3.5
- log_decay: float32 [2, 16, 8192], P(None, 'tp', 'sp'), may hold values from -1.2 to 0, as said below
- head_gain: float32 [1024], P('tp'), may hold values from 0.1 to 1.9
- conv_output: bfloat16 [1024, 2048], P('tp', 'sp'), may hold values from -0.1875 to 0.1875
- retention_output: bfloat16 [1024, 2048], P('tp', 'sp'), may hold values from -0.1875 to 0.1875
Outputs:
- mixed: bfloat16 [8192, 2048], P(('sp', 'tp'))
Inputs may be any that keep to these rules, and one draw needn't show every extreme that they name: `log_decay`: logarithms of per-position decays, below zero.
All inputs are finite; a program needn't handle non-finite values.
Results may differ from a plain program's by a relative error of at most 0.02.
Values may be sent and summed in bfloat16 or wider, within the bound.
A program may use at most 128 MiB of HBM per device.

v0:
```python
import jax
import jax.numpy as jnp
from jax import lax
from jax.sharding import PartitionSpec as P

HEAD_DIM = 64
EPS = 1e-06
THETA = 10000.0


def with_halo(shard, sides, width):
    for axis, dim in sides:
        size, length = (lax.axis_size(axis), shard.shape[dim])
        up = [(i, (i + 1) % size) for i in range(size - 1)]
        down = [(j, i) for i, j in up]
        last = lax.slice_in_dim(shard, length - width, length, axis=dim)
        first = lax.slice_in_dim(shard, 0, width, axis=dim)
        before = lax.ppermute(last, axis, up)
        after = lax.ppermute(first, axis, down)
        shard = jnp.concatenate([before, shard, after], axis=dim)
    return shard


def rotate(field_in, position_list):
    half_dim = field_in.shape[-1] // 2
    frequency = jnp.exp(
        -jnp.log(THETA) * jnp.arange(half_dim, dtype=jnp.float32) * (2.0 / field_in.shape[-1])
    )
    angles = position_list.astype(jnp.float32)[:, None, None] * frequency
    cosine = jnp.cos(angles)
    sine_part = jnp.sin(angles)
    leading = field_in[..., :half_dim]
    trailing = field_in[..., half_dim:]
    return jnp.concatenate(
        [leading * cosine - trailing * sine_part, leading * sine_part + trailing * cosine], axis=-1
    )


def conv_branch(outer_rows, inner_rows, conv_values, conv_taps):
    inner_value = (inner_rows.astype(jnp.float32) * conv_values.astype(jnp.float32)).astype(
        jnp.bfloat16
    )
    padded = with_halo(inner_value, (("sp", 0),), 1).astype(jnp.float32)
    convolved = conv_taps[0] * padded[:-2] + conv_taps[1] * padded[1:-1] + conv_taps[2] * padded[2:]
    return (outer_rows.astype(jnp.float32) * convolved).astype(jnp.bfloat16)


def span_parts(query_rows, key_rows, value_rows, log_rates):
    length = query_rows.shape[0]
    forward_cum = jnp.cumsum(log_rates[0], axis=-1)
    backward_cum = jnp.flip(jnp.cumsum(jnp.flip(log_rates[1], -1), axis=-1), -1)
    row_index = lax.broadcasted_iota(jnp.int32, (length, length), 0)
    col_index = lax.broadcasted_iota(jnp.int32, (length, length), 1)
    lower_part = (col_index <= row_index)[None]
    spread = jnp.where(
        lower_part,
        forward_cum[:, :, None] - forward_cum[:, None, :],
        backward_cum[:, :, None] - backward_cum[:, None, :],
    )
    scores = jnp.einsum("ihe,jhe->hij", query_rows, key_rows, preferred_element_type=jnp.float32)
    weighted = (scores * jnp.exp(spread)).astype(jnp.bfloat16)
    local_part = jnp.einsum(
        "hij,jhe->ihe", weighted, value_rows, preferred_element_type=jnp.float32
    )
    key_wide = key_rows.astype(jnp.float32)
    forward_keys = (key_wide * jnp.exp(forward_cum[:, -1:] - forward_cum).T[:, :, None]).astype(
        jnp.bfloat16
    )
    backward_keys = (key_wide * jnp.exp(backward_cum[:, :1] - backward_cum).T[:, :, None]).astype(
        jnp.bfloat16
    )
    forward_state = jnp.einsum(
        "jhd,jhe->hde", forward_keys, value_rows, preferred_element_type=jnp.float32
    )
    backward_state = jnp.einsum(
        "jhd,jhe->hde", backward_keys, value_rows, preferred_element_type=jnp.float32
    )
    return (local_part, forward_cum, backward_cum, forward_state, backward_state)


def retention_branch(query_rows, key_rows, value_rows, gate_rows, log_decay, head_gain, offsets):
    row_count = query_rows.shape[0]
    head_count = query_rows.shape[1] // HEAD_DIM
    shape_heads = (row_count, head_count, HEAD_DIM)
    rotated_query = rotate(query_rows.astype(jnp.float32).reshape(shape_heads), offsets).astype(
        jnp.bfloat16
    )
    rotated_key = (
        rotate(key_rows.astype(jnp.float32).reshape(shape_heads), offsets) * HEAD_DIM ** (-0.5)
    ).astype(jnp.bfloat16)
    local_part, forward_cum, backward_cum, forward_state, backward_state = span_parts(
        rotated_query, rotated_key, value_rows.reshape(shape_heads), log_decay
    )
    forward_total = forward_cum[:, -1]
    backward_total = backward_cum[:, 0]
    totals = lax.all_gather(
        jnp.stack([forward_total, backward_total])[None], "sp", axis=0, tiled=True
    )
    inclusive = jnp.cumsum(totals, axis=0)
    exclusive = inclusive - totals
    own_index = lax.axis_index("sp")
    own_inclusive = lax.dynamic_index_in_dim(inclusive, own_index, 0, keepdims=False)
    own_exclusive = lax.dynamic_index_in_dim(exclusive, own_index, 0, keepdims=False)
    pieces = (
        lax.all_gather(forward_state[None], "sp", axis=0, tiled=True),
        lax.all_gather(backward_state[None], "sp", axis=0, tiled=True),
    )
    piece_count = pieces[0].shape[0]
    span_index = lax.iota(jnp.int32, piece_count)
    forward_weight = jnp.where(
        (span_index < own_index)[:, None],
        jnp.exp(jnp.minimum(own_exclusive[0] - inclusive[:, 0], 0.0)),
        0.0,
    )
    backward_weight = jnp.where(
        (span_index > own_index)[:, None],
        jnp.exp(jnp.minimum(exclusive[:, 1] - own_inclusive[1], 0.0)),
        0.0,
    )
    into_forward = jnp.einsum(
        "nh,nhde->hde", forward_weight, pieces[0], precision=lax.Precision.HIGHEST
    )
    into_backward = jnp.einsum(
        "nh,nhde->hde", backward_weight, pieces[1], precision=lax.Precision.HIGHEST
    )
    forward_part = jnp.einsum(
        "ihd,hde->ihe",
        rotated_query,
        into_forward.astype(jnp.bfloat16),
        preferred_element_type=jnp.float32,
    )
    backward_part = jnp.einsum(
        "ihd,hde->ihe",
        rotated_query,
        into_backward.astype(jnp.bfloat16),
        preferred_element_type=jnp.float32,
    )
    mixed_heads = (
        local_part
        + jnp.exp(forward_cum).T[:, :, None] * forward_part
        + jnp.exp(backward_cum).T[:, :, None] * backward_part
    )
    scaled = mixed_heads * lax.rsqrt(
        jnp.mean(mixed_heads * mixed_heads, axis=-1, keepdims=True) + EPS
    )
    scaled = scaled * head_gain.reshape(head_count, HEAD_DIM)
    return (
        jax.nn.silu(gate_rows.astype(jnp.float32))
        * scaled.reshape(row_count, head_count * HEAD_DIM)
    ).astype(jnp.bfloat16)


def local(
    tokens,
    norm_gain,
    outer_gate,
    inner_gate,
    conv_input,
    query_proj,
    key_proj,
    value_proj,
    out_gate,
    conv_taps,
    log_decay,
    head_gain,
    conv_output,
    retention_output,
):
    whole = lax.all_gather(tokens, "tp", axis=1, tiled=True)
    wide = whole.astype(jnp.float32)
    normed = (
        wide * lax.rsqrt(jnp.mean(wide * wide, axis=-1, keepdims=True) + EPS) * norm_gain
    ).astype(jnp.bfloat16)
    row_count = normed.shape[0]
    offsets = lax.axis_index("sp") * row_count + lax.iota(jnp.int32, row_count)
    gathered = (
        lax.all_gather(outer_gate, "sp", axis=0, tiled=True),
        lax.all_gather(inner_gate, "sp", axis=0, tiled=True),
        lax.all_gather(conv_input, "sp", axis=0, tiled=True),
        lax.all_gather(query_proj, "sp", axis=0, tiled=True),
        lax.all_gather(key_proj, "sp", axis=0, tiled=True),
        lax.all_gather(value_proj, "sp", axis=0, tiled=True),
        lax.all_gather(out_gate, "sp", axis=0, tiled=True),
        lax.all_gather(conv_output, "sp", axis=1, tiled=True),
        lax.all_gather(retention_output, "sp", axis=1, tiled=True),
    )
    projected = [
        jnp.dot(normed, weight, preferred_element_type=jnp.float32).astype(jnp.bfloat16)
        for weight in gathered[:7]
    ]
    conv_out = conv_branch(projected[0], projected[1], projected[2], conv_taps)
    ret_out = retention_branch(
        projected[3], projected[4], projected[5], projected[6], log_decay, head_gain, offsets
    )
    conv_weight = gathered[7]
    ret_weight = gathered[8]
    return lax.psum_scatter(
        (
            jnp.dot(conv_out, conv_weight, preferred_element_type=jnp.float32)
            + jnp.dot(ret_out, ret_weight, preferred_element_type=jnp.float32)
        ).astype(jnp.bfloat16),
        "tp",
        scatter_dimension=0,
        tiled=True,
    )


def solution(mesh):
    return jax.shard_map(
        local,
        mesh=mesh,
        in_specs=(
            P("sp", "tp"),
            P(),
            P("sp", "tp"),
            P("sp", "tp"),
            P("sp", "tp"),
            P("sp", "tp"),
            P("sp", "tp"),
            P("sp", "tp"),
            P("sp", "tp"),
            P(None, "tp"),
            P(None, "tp", "sp"),
            P("tp"),
            P("tp", "sp"),
            P("tp", "sp"),
        ),
        out_specs=P(("sp", "tp"), None),
        check_vma=False,
    )
```

profile of v0, /device:TPU:0, one launch (start us, length us, event | category | flops | bytes accessed | tf_op | source)
XLA Modules:
  0.0 762.5 jit_solution(9898685039781030391)
XLA Ops:
  14.8 7.4 all-gather.17.cloned.1.call-done
  22.2 2.2 fusion
  24.4 62.1 %all-gather.31.cloned.1.call-done = bf16[2048,512]{1,0:T(8,128)(2,1)} async-done(((bf16[128,512]{1,0:T(8,128)(2,1)}), bf16[2048,512]{1,0:T(8,128)(2,1)}) %all-gather.31.cloned.1.call-update) | async-done | bytes 2097168 | tf_op jit(solution)/shard_map/all_gather | solution.py:180
  86.6 3.0 convolution_convert_fusion.1
  89.7 58.9 %all-gather.33.cloned.1.call-done = bf16[2048,512]{1,0:T(8,128)(2,1)} async-done(((bf16[128,512]{1,0:T(8,128)(2,1)}), bf16[2048,512]{1,0:T(8,128)(2,1)}) %all-gather.33.cloned.1.call-update) | async-done | bytes 2097168 | tf_op jit(solution)/shard_map/all_gather | solution.py:181
  148.6 3.6 convolution_convert_fusion
  152.3 1.2 multiply_subtract_fusion
  153.4 56.9 %all-gather.29.cloned.1.call-done = bf16[2048,512]{1,0:T(8,128)(2,1)} async-done(((bf16[128,512]{1,0:T(8,128)(2,1)}), bf16[2048,512]{1,0:T(8,128)(2,1)}) %all-gather.29.cloned.1.call-update) | async-done | bytes 2097168 | tf_op jit(solution)/shard_map/all_gather | solution.py:182
  210.4 3.6 convolution_convert_fusion.2
  218.2 2.2 fusion.34
  221.9 38.7 %all-gather.3 = f32[16,2,8]{2,1,0:T(2,128)S(1)} all-gather(f32[1,2,8]{2,1,0:T(2,128)S(1)} %maximum_bitcast_fusion), channel_id=2, replica_groups=mesh['sp'=16,'tp'=2] {'sp'}, dimensions={0}, use_global_device_ids=true | all-gather | bytes 1088 | tf_op jit(solution)/shard_map/all_gather | solution.py:96
  261.0 11.3 %all-gather.21.cloned.1.call-done = bf16[2048,512]{1,0:T(8,128)(2,1)} async-done(((bf16[128,512]{1,0:T(8,128)(2,1)}), bf16[2048,512]{1,0:T(8,128)(2,1)}) %all-gather.21.cloned.1.call-update) | async-done | bytes 2097168 | tf_op jit(solution)/shard_map/all_gather | solution.py:178
  272.3 3.9 fusion.18
  276.2 58.0 %all-gather.23.cloned.1.call-done = bf16[2048,512]{1,0:T(8,128)(2,1)} async-done(((bf16[128,512]{1,0:T(8,128)(2,1)}), bf16[2048,512]{1,0:T(8,128)(2,1)}) %all-gather.23.cloned.1.call-update) | async-done | bytes 2097168 | tf_op jit(solution)/shard_map/all_gather | solution.py:179
  334.2 3.2 fusion.22
  337.4 3.2 collective-permute-start
  340.5 1.5 collective-permute-start.1
  342.0 5.8 fusion.11
  347.8 1.2 maximum_convert_fusion
  349.0 47.2 %all-gather.19.cloned.1.call-done = bf16[2048,512]{1,0:T(8,128)(2,1)} async-done(((bf16[128,512]{1,0:T(8,128)(2,1)}), bf16[2048,512]{1,0:T(8,128)(2,1)}) %all-gather.19.cloned.1.call-update) | async-done | bytes 2097168 | tf_op jit(solution)/shard_map/all_gather | solution.py:177
  396.2 64.5 %all-gather.25.cloned.1.call-done = bf16[512,2048]{1,0:T(8,128)(2,1)} async-done(((bf16[512,128]{1,0:T(8,128)(2,1)}), bf16[512,2048]{1,0:T(8,128)(2,1)}) %all-gather.25.cloned.1.call-update) | async-done | bytes 2097168 | tf_op jit(solution)/shard_map/all_gather | solution.py:184
  460.7 7.7 %fusion.33 = f32[512,2048]{1,0:T(8,128)} fusion(bf16[512,2048]{1,0:T(8,128)(2,1)} %all-gather.25.cloned.1.call-done, bf16[2048,512]{1,0:T(8,128)(2,1)} %all-gather.19.cloned.1.call-done, f32[514,512]{1,0:T(8,128)} %maximum_convert_fusion, f32[512]{0:T(512)S(1)} %bitcast.107, f32[512]{0:T(512)S(1)} %bitcast.108, f32[512]{0:T(512)S(1)} %bitcast.106, ...), kind=kOutput, calls=%fused_computation.56 | convolution fusion | flops 2154037248 | bytes 13647872 | tf_op jit(solution)/shard_map/dot_general | solution.py:199
  468.4 68.8 %all-gather.37.cloned.1.call-done = f32[128,64,64]{2,1,0:T(8,128)} async-done(((f32[8,64,64]{2,1,0:T(8,128)}), f32[128,64,64]{2,1,0:T(8,128)}) %all-gather.37.cloned.1.call-update) | async-done | bytes 2097168 | tf_op jit(solution)/shard_map/all_gather | solution.py:105
  537.2 6.4 fusion.5
  543.8 70.3 %all-gather.39.cloned.1.call-done = f32[128,64,64]{2,1,0:T(8,128)} async-done(((f32[8,64,64]{2,1,0:T(8,128)}), f32[128,64,64]{2,1,0:T(8,128)}) %all-gather.39.cloned.1.call-update) | async-done | bytes 2097168 | tf_op jit(solution)/shard_map/all_gather | solution.py:106
  614.1 6.6 fusion.3
  620.9 1.5 fusion.15
  622.9 1.3 copy.34
  624.2 51.7 %all-gather.27.cloned.1.call-done = bf16[2048,512]{1,0:T(8,128)(2,1)} async-done(((bf16[128,512]{1,0:T(8,128)(2,1)}), bf16[2048,512]{1,0:T(8,128)(2,1)}) %all-gather.27.cloned.1.call-update) | async-done | bytes 2097168 | tf_op jit(solution)/shard_map/all_gather | solution.py:183
  675.9 64.3 %all-gather.35.cloned.1.call-done = bf16[512,2048]{1,0:T(8,128)(2,1)} async-done(((bf16[512,128]{1,0:T(8,128)(2,1)}), bf16[512,2048]{1,0:T(8,128)(2,1)}) %all-gather.35.cloned.1.call-update) | async-done | bytes 2097168 | tf_op jit(solution)/shard_map/all_gather | solution.py:185
  740.2 7.6 %add_convert_fusion = bf16[512,2048]{1,0:T(8,128)(2,1)} fusion(f32[512,2048]{1,0:T(8,128)} %fusion.33, bf16[512,2048]{1,0:T(8,128)(2,1)} %all-gather.35.cloned.1.call-done, f32[512,512]{1,0:T(8,128)} %copy.34, bf16[2048,512]{1,0:T(8,128)(2,1)} %all-gather.27.cloned.1.call-done, bf16[512,2048]{1,0:T(8,128)(2,1)S(1)} %copy-done.1, f32[2048]{0:T(1024)S(1)} %copy-done.6, ...), kind=kOutput, calls=%fused_computation.10 | convolution fusion | flops 2155872256 | bytes 13641728 | tf_op jit(solution)/shard_map/dot_general | solution.py:200
  747.9 8.1 %reduce-scatter.2.cloned.1.call-done = bf16[256,2048]{1,0:T(8,128)(2,1)} async-done(((bf16[512,2048]{1,0:T(8,128)(2,1)}), bf16[256,2048]{1,0:T(8,128)(2,1)}) %reduce-scatter.2.cloned.1.call-update) | async-done | bytes 1048592 | tf_op jit(solution)/shard_map/reduce_scatter | solution.py:197
  (90 shorter events, 15.1 us)
Async XLA Ops:
  6.5 80.0 %copy-start.6 = (f32[2048]{0:T(1024)S(1)}, f32[2048]{0:T(1024)}, u32[]{:S(2)}) copy-start(f32[2048]{0:T(1024)} %param.15) | copy-start | bytes 24580
  6.5 15.7 %all-gather.17.cloned.1.call-start = ((), (), s32[]{:S(2)}) async-start(), calls=%async_computation.1 | async-start | bytes 3145728 | tf_op jit(solution)/shard_map/all_gather | solution.py:169
  7.3 79.3 %all-gather.31.cloned.1.call-start = ((), (), s32[]{:S(2)}) async-start(), calls=%async_computation.8 | async-start | bytes 2228224 | tf_op jit(solution)/shard_map/all_gather | solution.py:180
  8.0 140.5 %all-gather.33.cloned.1.call-start = ((), (), s32[]{:S(2)}) async-start(), calls=%async_computation.9 | async-start | bytes 2228224 | tf_op jit(solution)/shard_map/all_gather | solution.py:181
  8.7 201.6 %all-gather.29.cloned.1.call-start = ((), (), s32[]{:S(2)}) async-start(), calls=%async_computation.7 | async-start | bytes 2228224 | tf_op jit(solution)/shard_map/all_gather | solution.py:182
  9.3 263.0 %all-gather.21.cloned.1.call-start = ((), (), s32[]{:S(2)}) async-start(), calls=%async_computation.3 | async-start | bytes 2228224 | tf_op jit(solution)/shard_map/all_gather | solution.py:178
  9.9 324.3 %all-gather.23.cloned.1.call-start = ((), (), s32[]{:S(2)}) async-start(), calls=%async_computation.4 | async-start | bytes 2228224 | tf_op jit(solution)/shard_map/all_gather | solution.py:179
  10.5 385.7 %all-gather.19.cloned.1.call-start = ((), (), s32[]{:S(2)}) async-start(), calls=%async_computation.2 | async-start | bytes 2228224 | tf_op jit(solution)/shard_map/all_gather | solution.py:177
  11.2 449.4 %all-gather.25.cloned.1.call-start = ((), (), s32[]{:S(2)}) async-start(), calls=%async_computation.5 | async-start | bytes 2228224 | tf_op jit(solution)/shard_map/all_gather | solution.py:184
  12.0 525.3 %all-gather.37.cloned.1.call-start = ((), (), s32[]{:S(2)}) async-start(), calls=%async_computation.12 | async-start | bytes 4456448 | tf_op jit(solution)/shard_map/all_gather | solution.py:105
  22.2 64.4 %copy-start = (bf16[512,2048]{1,0:T(8,128)(2,1)S(1)}, bf16[512,2048]{1,0:T(8,128)(2,1)}, u32[]{:S(2)}) copy-start(bf16[512,2048]{1,0:T(8,128)(2,1)} %all-gather.17.cloned.1.call-done) | copy-start | bytes 6291460
  153.4 64.7 %copy-start.2 = (f32[512,8,32]{0,2,1:T(8,128)}, f32[512,8,32]{0,2,1:T(8,128)S(1)}, u32[]{:S(2)}) copy-start(f32[512,8,32]{0,2,1:T(8,128)S(1)} %get-tuple-element.7) | copy-start | bytes 1572868
  153.4 61.3 %copy-start.3 = (f32[512,8,32]{0,2,1:T(8,128)S(1)}, f32[512,8,32]{0,2,1:T(8,128)}, u32[]{:S(2)}) copy-start(f32[512,8,32]{0,2,1:T(8,128)} %get-tuple-element.8) | copy-start | bytes 1572868
  214.0 0.8 copy-start.7
  215.8 45.0 %copy-start.5 = (f32[512]{0:T(512)S(1)}, f32[512]{0:T(512)}, u32[]{:S(2)}) copy-start(f32[512]{0:T(512)} %param.25) | copy-start | bytes 6148
  215.8 45.1 %copy-start.4 = (f32[3,512]{1,0:T(4,128)S(1)}, f32[3,512]{1,0:T(4,128)}, u32[]{:S(2)}) copy-start(f32[3,512]{1,0:T(4,128)} %param.23) | copy-start | bytes 18436
  215.8 56.5 %copy-start.1 = (bf16[512,2048]{1,0:T(8,128)(2,1)S(1)}, bf16[512,2048]{1,0:T(8,128)(2,1)}, u32[]{:S(2)}) copy-start(bf16[512,2048]{1,0:T(8,128)(2,1)} %all-gather.17.cloned.1.call-done) | copy-start | bytes 6291460
  215.8 398.2 %all-gather.39.cloned.1.call-start = ((), (), s32[]{:S(2)}) async-start(), calls=%async_computation.13 | async-start | bytes 4456448 | tf_op jit(solution)/shard_map/all_gather | solution.py:106
  220.4 455.5 %all-gather.27.cloned.1.call-start = ((), (), s32[]{:S(2)}) async-start(), calls=%async_computation.6 | async-start | bytes 2228224 | tf_op jit(solution)/shard_map/all_gather | solution.py:183
  221.1 519.1 %all-gather.35.cloned.1.call-start = ((), (), s32[]{:S(2)}) async-start(), calls=%async_computation.10 | async-start | bytes 2228224 | tf_op jit(solution)/shard_map/all_gather | solution.py:185
  221.7 534.2 %reduce-scatter.2.cloned.1.call-start = ((), (), s32[]{:S(2)}) async-start(), calls=%async_computation.11 | async-start | bytes 3145728 | tf_op jit(solution)/shard_map/reduce_scatter | solution.py:197
  337.4 10.4 %collective-permute-start = (bf16[1,512]{1,0:T(2,128)(2,1)S(1)}, bf16[1,512]{1,0:T(2,128)(2,1)S(1)}, u32[]{:S(2)}, u32[]{:S(2)}) collective-permute-start(bf16[1,512]{1,0:T(2,128)(2,1)S(1)} %get-tuple-element.11), channel_id=1, source_target_pairs={{0,2},{2,4},{4,6},{6,8},{8,10},{10,12},{12,14},{14,16},{16,18},{18... | collective-permute-start | bytes 3080 | tf_op jit(solution)/shard_map/ppermute | solution.py:18
  340.5 7.3 collective-permute-start.1
Sparse Core Ops, SparseCore 0:
  8.9 13.2 all-gather.16
  25.0 61.5 all-gather.30
  89.3 59.1 all-gather.32
  151.2 59.1 all-gather.28
  213.0 59.2 all-gather.20
  275.0 59.1 all-gather.22
  336.9 59.1 all-gather.18
  398.9 61.7 all-gather.24
  463.4 73.7 all-gather.36
  539.9 74.1 all-gather.38
  616.9 58.9 all-gather.26
  678.4 61.7 all-gather.34
  748.0 7.9 reduce-scatter.1
where the time goes:
time: 763 us; the launch traced here: 762 us
  waiting for transfers between devices  636 us (83%)
  matrix products  56.5 us (7%)
  blocking collectives  38.7 us (5%)
  between operations  13.5 us (2%)
  other arithmetic  8.18 us (1%)
    all_gather x1, waiting for transfers between devices, retention_branch(): lax.all_gather(backward_state[None], 'sp', axis=0, tiled=True)  70.3 us
    all_gather x1, waiting for transfers between devices, retention_branch(): lax.all_gather(forward_state[None], 'sp', axis=0, tiled=True)  68.8 us
    all_gather x1, waiting for transfers between devices, local(): lax.all_gather(conv_output, 'sp', axis=1, tiled=True)  64.5 us
    all_gather x1, waiting for transfers between devices, local(): lax.all_gather(retention_output, 'sp', axis=1, tiled=True)  64.3 us
    all_gather x1, waiting for transfers between devices, local(): lax.all_gather(query_proj, 'sp', axis=0, tiled=True)  62.1 us
    all_gather x1, waiting for transfers between devices, local(): lax.all_gather(key_proj, 'sp', axis=0, tiled=True)  58.9 us
    all_gather x1, waiting for transfers between devices, local(): lax.all_gather(conv_input, 'sp', axis=0, tiled=True)  58 us
    all_gather x1, waiting for transfers between devices, local(): lax.all_gather(value_proj, 'sp', axis=0, tiled=True)  56.9 us
  transfers between devices with their start and end apart: 15, of which 13 were waited for; matrix products, arithmetic and copies ran while one was open for 8% of the time, Pallas kernels for 0%

commit v1 on v0

--- a/solution.py
+++ b/solution.py
@@ -182,7 +182,7 @@
         lax.all_gather(value_proj, "sp", axis=0, tiled=True),
         lax.all_gather(out_gate, "sp", axis=0, tiled=True),
         lax.all_gather(conv_output, "sp", axis=1, tiled=True),
-        lax.all_gather(retention_output, "sp", axis=1, tiled=True),
+        jnp.concatenate(lax.all_gather(retention_output, "sp"), axis=1),
     )
     projected = [
         jnp.dot(normed, weight, preferred_element_type=jnp.float32).astype(jnp.bfloat16)

time: 763 us -> 761 us (level)
    all_gather x1, waiting for transfers between devices: 64.3 us -> 48.4 us  [local(): lax.all_gather(retention_output, 'sp')]
    all_gather x1, waiting for transfers between devices: 47.2 us -> 56.9 us  [local(): lax.all_gather(outer_gate, 'sp', axis=0, tiled=True)]
where the time goes in v1:
time: 761 us; the launch traced here: 760 us
  waiting for transfers between devices  631 us (83%)
  matrix products  56.3 us (7%)
  blocking collectives  38.6 us (5%)
  between operations  13.5 us (2%)
  other arithmetic  8.2 us (1%)
  local copies, waits for them, and re-layouts  7.87 us (1%)
    all_gather x1, waiting for transfers between devices, retention_branch(): lax.all_gather(backward_state[None], 'sp', axis=0, tiled=True)  70.4 us
    all_gather x1, waiting for transfers between devices, retention_branch(): lax.all_gather(forward_state[None], 'sp', axis=0, tiled=True)  68.7 us
    all_gather x1, waiting for transfers between devices, local(): lax.all_gather(conv_output, 'sp', axis=1, tiled=True)  64.5 us
    all_gather x1, waiting for transfers between devices, local(): lax.all_gather(query_proj, 'sp', axis=0, tiled=True)  62.1 us
    all_gather x1, waiting for transfers between devices, local(): lax.all_gather(key_proj, 'sp', axis=0, tiled=True)  58.9 us
    all_gather x1, waiting for transfers between devices, local(): lax.all_gather(conv_input, 'sp', axis=0, tiled=True)  58 us
    all_gather x1, waiting for transfers between devices, local(): lax.all_gather(value_proj, 'sp', axis=0, tiled=True)  56.9 us
    all_gather x1, waiting for transfers between devices, local(): lax.all_gather(outer_gate, 'sp', axis=0, tiled=True)  56.9 us
  transfers between devices with their start and end apart: 15, of which 13 were waited for; matrix products, arithmetic and copies ran while one was open for 8% of the time, Pallas kernels for 0%

profile of v1, /device:TPU:0, one launch (start us, length us, event | category | flops | bytes accessed | tf_op | source)
XLA Modules:
  0.0 760.5 jit_solution(4519337541063496447)
XLA Ops:
  14.8 7.4 all-gather.18.cloned.1.call-done
  22.2 2.2 fusion
  24.4 62.1 %all-gather.32.cloned.1.call-done = bf16[2048,512]{1,0:T(8,128)(2,1)} async-done(((bf16[128,512]{1,0:T(8,128)(2,1)}), bf16[2048,512]{1,0:T(8,128)(2,1)}) %all-gather.32.cloned.1.call-update) | async-done | bytes 2097168 | tf_op jit(solution)/shard_map/all_gather | solution.py:180
  86.6 3.0 convolution_convert_fusion.1
  89.7 58.9 %all-gather.34.cloned.1.call-done = bf16[2048,512]{1,0:T(8,128)(2,1)} async-done(((bf16[128,512]{1,0:T(8,128)(2,1)}), bf16[2048,512]{1,0:T(8,128)(2,1)}) %all-gather.34.cloned.1.call-update) | async-done | bytes 2097168 | tf_op jit(solution)/shard_map/all_gather | solution.py:181
  148.6 3.6 convolution_convert_fusion
  153.5 56.9 %all-gather.30.cloned.1.call-done = bf16[2048,512]{1,0:T(8,128)(2,1)} async-done(((bf16[128,512]{1,0:T(8,128)(2,1)}), bf16[2048,512]{1,0:T(8,128)(2,1)}) %all-gather.30.cloned.1.call-update) | async-done | bytes 2097168 | tf_op jit(solution)/shard_map/all_gather | solution.py:182
  210.4 3.6 convolution_convert_fusion.2
  218.2 2.2 fusion.34
  221.2 38.6 %all-gather.4 = f32[16,2,8]{2,1,0:T(2,128)S(1)} all-gather(f32[1,2,8]{2,1,0:T(2,128)S(1)} %maximum_bitcast_fusion), channel_id=2, replica_groups=mesh['sp'=16,'tp'=2] {'sp'}, dimensions={0}, use_global_device_ids=true | all-gather | bytes 1088 | tf_op jit(solution)/shard_map/all_gather | solution.py:96
  260.3 11.9 %all-gather.22.cloned.1.call-done = bf16[2048,512]{1,0:T(8,128)(2,1)} async-done(((bf16[128,512]{1,0:T(8,128)(2,1)}), bf16[2048,512]{1,0:T(8,128)(2,1)}) %all-gather.22.cloned.1.call-update) | async-done | bytes 2097168 | tf_op jit(solution)/shard_map/all_gather | solution.py:178
  272.2 3.9 fusion.18
  276.1 58.0 %all-gather.24.cloned.1.call-done = bf16[2048,512]{1,0:T(8,128)(2,1)} async-done(((bf16[128,512]{1,0:T(8,128)(2,1)}), bf16[2048,512]{1,0:T(8,128)(2,1)}) %all-gather.24.cloned.1.call-update) | async-done | bytes 2097168 | tf_op jit(solution)/shard_map/all_gather | solution.py:179
  334.0 3.2 fusion.22
  337.2 3.2 collective-permute-start
  340.4 1.5 collective-permute-start.1
  341.9 5.8 fusion.11
  347.6 48.4 %all-gather.40.cloned.1.call-done = bf16[8192,128]{1,0:T(8,128)(2,1)} async-done(((bf16[512,128]{1,0:T(8,128)(2,1)}), bf16[8192,128]{1,0:T(8,128)(2,1)}) %all-gather.40.cloned.1.call-update) | async-done | bytes 2097168 | tf_op jit(solution)/shard_map/all_gather | solution.py:185
  396.0 3.9 copy.36
  400.0 1.2 maximum_convert_fusion
  401.1 56.9 %all-gather.20.cloned.1.call-done = bf16[2048,512]{1,0:T(8,128)(2,1)} async-done(((bf16[128,512]{1,0:T(8,128)(2,1)}), bf16[2048,512]{1,0:T(8,128)(2,1)}) %all-gather.20.cloned.1.call-update) | async-done | bytes 2097168 | tf_op jit(solution)/shard_map/all_gather | solution.py:177
  458.0 64.5 %all-gather.26.cloned.1.call-done = bf16[512,2048]{1,0:T(8,128)(2,1)} async-done(((bf16[512,128]{1,0:T(8,128)(2,1)}), bf16[512,2048]{1,0:T(8,128)(2,1)}) %all-gather.26.cloned.1.call-update) | async-done | bytes 2097168 | tf_op jit(solution)/shard_map/all_gather | solution.py:184
  522.5 7.7 %fusion.33 = f32[512,2048]{1,0:T(8,128)} fusion(bf16[512,2048]{1,0:T(8,128)(2,1)} %all-gather.26.cloned.1.call-done, bf16[2048,512]{1,0:T(8,128)(2,1)} %all-gather.20.cloned.1.call-done, f32[514,512]{1,0:T(8,128)} %maximum_convert_fusion, f32[512]{0:T(512)S(1)} %bitcast.113, f32[512]{0:T(512)S(1)} %bitcast.114, f32[512]{0:T(512)S(1)} %bitcast.112, ...), kind=kOutput, calls=%fused_computation.56 | convolution fusion | flops 2154037248 | bytes 13647872 | tf_op jit(solution)/shard_map/dot_general | solution.py:199
  530.2 68.7 %all-gather.36.cloned.1.call-done = f32[128,64,64]{2,1,0:T(8,128)} async-done(((f32[8,64,64]{2,1,0:T(8,128)}), f32[128,64,64]{2,1,0:T(8,128)}) %all-gather.36.cloned.1.call-update) | async-done | bytes 2097168 | tf_op jit(solution)/shard_map/all_gather | solution.py:105
  598.9 6.4 fusion.5
  605.5 70.4 %all-gather.38.cloned.1.call-done = f32[128,64,64]{2,1,0:T(8,128)} async-done(((f32[8,64,64]{2,1,0:T(8,128)}), f32[128,64,64]{2,1,0:T(8,128)}) %all-gather.38.cloned.1.call-update) | async-done | bytes 2097168 | tf_op jit(solution)/shard_map/all_gather | solution.py:106
  675.9 6.4 fusion.3
  682.5 1.5 fusion.15
  684.5 1.3 copy.35
  685.8 51.8 %all-gather.28.cloned.1.call-done = bf16[2048,512]{1,0:T(8,128)(2,1)} async-done(((bf16[128,512]{1,0:T(8,128)(2,1)}), bf16[2048,512]{1,0:T(8,128)(2,1)}) %all-gather.28.cloned.1.call-update) | async-done | bytes 2097168 | tf_op jit(solution)/shard_map/all_gather | solution.py:183
  737.6 7.6 %add_convert_fusion = bf16[512,2048]{1,0:T(8,128)(2,1)} fusion(f32[512,2048]{1,0:T(8,128)} %fusion.33, bf16[512,2048]{0,1:T(8,128)(2,1)} %bitcast.104, f32[512,512]{1,0:T(8,128)} %copy.35, bf16[2048,512]{1,0:T(8,128)(2,1)} %all-gather.28.cloned.1.call-done, bf16[512,2048]{1,0:T(8,128)(2,1)S(1)} %copy-done.1, f32[2048]{0:T(1024)S(1)} %copy-done.7, ...), kind=kOutput, calls=%fused_computation.10 | convolution fusion | flops 2155872256 | bytes 13641728 | tf_op jit(solution)/shard_map/dot_general | solution.py:200
  745.2 8.7 %reduce-scatter.2.cloned.1.call-done = bf16[256,2048]{1,0:T(8,128)(2,1)} async-done(((bf16[512,2048]{1,0:T(8,128)(2,1)}), bf16[256,2048]{1,0:T(8,128)(2,1)}) %reduce-scatter.2.cloned.1.call-update) | async-done | bytes 1048592 | tf_op jit(solution)/shard_map/reduce_scatter | solution.py:197
  (93 shorter events, 15.6 us)
Async XLA Ops:
  6.5 6.2 copy-start.4
  6.5 80.0 %copy-start.7 = (f32[2048]{0:T(1024)S(1)}, f32[2048]{0:T(1024)}, u32[]{:S(2)}) copy-start(f32[2048]{0:T(1024)} %param.15) | copy-start | bytes 24580
  6.5 15.7 %all-gather.18.cloned.1.call-start = ((), (), s32[]{:S(2)}) async-start(), calls=%async_computation.1 | async-start | bytes 3145728 | tf_op jit(solution)/shard_map/all_gather | solution.py:169
  7.3 79.3 %all-gather.32.cloned.1.call-start = ((), (), s32[]{:S(2)}) async-start(), calls=%async_computation.8 | async-start | bytes 2228224 | tf_op jit(solution)/shard_map/all_gather | solution.py:180
  8.0 140.5 %all-gather.34.cloned.1.call-start = ((), (), s32[]{:S(2)}) async-start(), calls=%async_computation.9 | async-start | bytes 2228224 | tf_op jit(solution)/shard_map/all_gather | solution.py:181
  8.7 201.6 %all-gather.30.cloned.1.call-start = ((), (), s32[]{:S(2)}) async-start(), calls=%async_computation.7 | async-start | bytes 2228224 | tf_op jit(solution)/shard_map/all_gather | solution.py:182
  9.3 262.9 %all-gather.22.cloned.1.call-start = ((), (), s32[]{:S(2)}) async-start(), calls=%async_computation.3 | async-start | bytes 2228224 | tf_op jit(solution)/shard_map/all_gather | solution.py:178
  9.9 324.1 %all-gather.24.cloned.1.call-start = ((), (), s32[]{:S(2)}) async-start(), calls=%async_computation.4 | async-start | bytes 2228224 | tf_op jit(solution)/shard_map/all_gather | solution.py:179
  10.5 385.6 %all-gather.40.cloned.1.call-start = ((), (), s32[]{:S(2)}) async-start(), calls=%async_computation.13 | async-start | bytes 2228224 | tf_op jit(solution)/shard_map/all_gather | solution.py:185
  11.2 446.8 %all-gather.20.cloned.1.call-start = ((), (), s32[]{:S(2)}) async-start(), calls=%async_computation.2 | async-start | bytes 2228224 | tf_op jit(solution)/shard_map/all_gather | solution.py:177
  12.0 510.5 %all-gather.26.cloned.1.call-start = ((), (), s32[]{:S(2)}) async-start(), calls=%async_computation.5 | async-start | bytes 2228224 | tf_op jit(solution)/shard_map/all_gather | solution.py:184
  12.7 586.2 %all-gather.36.cloned.1.call-start = ((), (), s32[]{:S(2)}) async-start(), calls=%async_computation.11 | async-start | bytes 4456448 | tf_op jit(solution)/shard_map/all_gather | solution.py:105
  22.2 64.4 %copy-start = (bf16[512,2048]{1,0:T(8,128)(2,1)S(1)}, bf16[512,2048]{1,0:T(8,128)(2,1)}, u32[]{:S(2)}) copy-start(bf16[512,2048]{1,0:T(8,128)(2,1)} %all-gather.18.cloned.1.call-done) | copy-start | bytes 6291460
  153.4 64.7 %copy-start.2 = (f32[512,8,32]{0,2,1:T(8,128)}, f32[512,8,32]{0,2,1:T(8,128)S(1)}, u32[]{:S(2)}) copy-start(f32[512,8,32]{0,2,1:T(8,128)S(1)} %get-tuple-element.7) | copy-start | bytes 1572868
  153.4 61.3 %copy-start.3 = (f32[512,8,32]{0,2,1:T(8,128)S(1)}, f32[512,8,32]{0,2,1:T(8,128)}, u32[]{:S(2)}) copy-start(f32[512,8,32]{0,2,1:T(8,128)} %get-tuple-element.8) | copy-start | bytes 1572868
  214.0 0.8 copy-start.8
  215.8 44.2 %copy-start.6 = (f32[512]{0:T(512)S(1)}, f32[512]{0:T(512)}, u32[]{:S(2)}) copy-start(f32[512]{0:T(512)} %param.25) | copy-start | bytes 6148
  215.8 44.2 %copy-start.5 = (f32[3,512]{1,0:T(4,128)S(1)}, f32[3,512]{1,0:T(4,128)}, u32[]{:S(2)}) copy-start(f32[3,512]{1,0:T(4,128)} %param.23) | copy-start | bytes 18436
  215.8 56.4 %copy-start.1 = (bf16[512,2048]{1,0:T(8,128)(2,1)S(1)}, bf16[512,2048]{1,0:T(8,128)(2,1)}, u32[]{:S(2)}) copy-start(bf16[512,2048]{1,0:T(8,128)(2,1)} %all-gather.18.cloned.1.call-done) | copy-start | bytes 6291460
  215.9 460.1 %all-gather.38.cloned.1.call-start = ((), (), s32[]{:S(2)}) async-start(), calls=%async_computation.12 | async-start | bytes 4456448 | tf_op jit(solution)/shard_map/all_gather | solution.py:106
  220.4 517.1 %all-gather.28.cloned.1.call-start = ((), (), s32[]{:S(2)}) async-start(), calls=%async_computation.6 | async-start | bytes 2228224 | tf_op jit(solution)/shard_map/all_gather | solution.py:183
  221.0 532.9 %reduce-scatter.2.cloned.1.call-start = ((), (), s32[]{:S(2)}) async-start(), calls=%async_computation.10 | async-start | bytes 3145728 | tf_op jit(solution)/shard_map/reduce_scatter | solution.py:197
  337.2 62.7 %collective-permute-start = (bf16[1,512]{1,0:T(2,128)(2,1)S(1)}, bf16[1,512]{1,0:T(2,128)(2,1)S(1)}, u32[]{:S(2)}, u32[]{:S(2)}) collective-permute-start(bf16[1,512]{1,0:T(2,128)(2,1)S(1)} %get-tuple-element.11), channel_id=1, source_target_pairs={{0,2},{2,4},{4,6},{6,8},{8,10},{10,12},{12,14},{14,16},{16,18},{18... | collective-permute-start | bytes 3080 | tf_op jit(solution)/shard_map/ppermute | solution.py:18
  340.4 59.6 %collective-permute-start.1 = (bf16[1,512]{1,0:T(2,128)(2,1)S(1)}, bf16[1,512]{1,0:T(2,128)(2,1)S(1)}, u32[]{:S(2)}, u32[]{:S(2)}) collective-permute-start(bf16[1,512]{1,0:T(2,128)(2,1)S(1)} %get-tuple-element.12), channel_id=1, source_target_pairs={{2,0},{4,2},{6,4},{8,6},{10,8},{12,10},{14,12},{16,14},{18,16},{20... | collective-permute-start | bytes 3080 | tf_op jit(solution)/shard_map/ppermute | solution.py:19
Sparse Core Ops, SparseCore 0:
  8.9 13.2 all-gather.17
  25.0 61.5 all-gather.31
  89.3 59.1 all-gather.33
  151.2 59.1 all-gather.29
  213.0 59.1 all-gather.21
  274.8 59.1 all-gather.23
  336.8 59.1 all-gather.39
  398.8 59.1 all-gather.19
  460.7 61.7 all-gather.25
  525.1 73.7 all-gather.35
  601.7 74.1 all-gather.37
  678.6 58.9 all-gather.27
  745.4 8.5 reduce-scatter.1
